TPU v7x, 32 devices: a whole 2x2x4 slice. The times are simulated.
32 devices in a mesh: sp: 8 (over z, y), tp: 4 (over x, core).
Axes of the slice: x: 2, y: 2, z: 4, core: 2. Of those that a mesh axis runs over, the one named last changes fastest.
Arguments:
- residual_entry_input: bfloat16 [8192, 2048], P(('sp', 'tp')), may hold values from -6 to 6
- query_matrix_rows: bfloat16 [8192, 1024], P('sp', 'tp'), may hold values from -6 to 6
- key_matrix_rows: bfloat16 [8192, 1024], P('sp', 'tp'), may hold values from -6 to 6
- value_matrix_rows: bfloat16 [8192, 2048], P('sp', 'tp'), may hold values from -6 to 6
- output_gate_logits: bfloat16 [8192, 2048], P('sp', 'tp'), may hold values from -6 to 6
- input_gate_logits: float32 [8192, 8], P('sp', 'tp'), may hold values from -6 to 6
- forget_gate_logits: float32 [8192, 8], P('sp', 'tp'), may hold values from -8 to 31
- forget_decay_offset: float32 [8192, 8], P('sp', 'tp'), may hold values from -0.7 to 0
- head_norm_gain: float32 [8, 256], P('tp'), may hold values from 0.1 to 1.9
- cell_output_weight: bfloat16 [2048, 2048], P('tp'), may hold values from -0.125 to 0.125
- feedforward_norm_gain: float32 [2048], replicated, may hold values from 0.1 to 1.9
- gate_up_weight: bfloat16 [2048, 5632], P('sp', 'tp'), may hold values from -0.125 to 0.125
- value_up_weight: bfloat16 [2048, 5632], P('sp', 'tp'), may hold values from -0.125 to 0.125
- gate_filter_taps: float32 [3, 5632], P(None, 'tp'), may hold values from -3 to 3
- value_filter_taps: float32 [3, 5632], P(None, 'tp'), may hold values from -3 to 3
- down_projection_weight: bfloat16 [5632, 2048], P('tp', 'sp'), may hold values from -0.078125 to 0.078125
Outputs:
- result: bfloat16 [8192, 2048], P(('sp', 'tp'))
All inputs are finite; a program needn't handle non-finite values.
Results may differ from a plain program's by a relative error of at most 0.025.
Values may be sent and summed in bfloat16 or wider, within the bound.
No kernel may reach another device: no remote copies, remote signals or barrier semaphores. Data moves between devices by JAX's collectives and lax.ppermute only.
A program may use at most 128 MiB of HBM per device.

v0:
```python
import jax
import jax.numpy as jnp
from jax import lax
from jax.sharding import PartitionSpec as P

BLOCK = 128
eps = 1e-06
neg_large = -1e30


def carried_in(x, axis, combine, identity):
    count, position = (lax.axis_size(axis), lax.axis_index(axis))
    everything = jax.tree.map(
        lambda part, kind: lax.all_gather(part.astype(kind), axis),
        x,
        (jnp.bfloat16, jnp.bfloat16, jnp.bfloat16, jnp.bfloat16),
    )
    start = jax.tree.map(
        lambda part, zero: jnp.broadcast_to(jnp.asarray(zero, part.dtype), part.shape), x, identity
    )

    def lap(k, before):
        reached = k < position
        new = combine(
            before, jax.tree.map(lambda part, own: part[k].astype(own.dtype), everything, x)
        )
        return jax.tree.map(lambda a, b: jnp.where(reached, a, b), new, before)

    return lax.fori_loop(0, count, lap, start)


def shifted(x, axis, by):
    count = lax.axis_size(axis)
    pairs = [(i, i + by) for i in range(count) if 0 <= i + by < count]
    return lax.ppermute(x, axis, pairs)


def gate_log_values(input_gate_logits, forget_gate_logits, forget_decay_offset):
    input_log_value = 15.0 * jnp.tanh(input_gate_logits / 15.0)
    forget_log_sigmoid = (
        jax.nn.log_sigmoid(15.0 * jnp.tanh(forget_gate_logits / 15.0)) + forget_decay_offset
    )
    return (input_log_value, forget_log_sigmoid)


def combine_states(earlier, later):
    total_one, memory_one, normer_one, running_one = earlier
    total_two, memory_two, normer_two, running_two = later
    joined = jnp.maximum(total_two + running_one, running_two)
    weight_one = jnp.exp(total_two + running_one - joined)
    weight_two = jnp.exp(running_two - joined)
    memory = weight_one[:, None, None] * memory_one + weight_two[:, None, None] * memory_two
    normer = weight_one[:, None] * normer_one + weight_two[:, None] * normer_two
    return (total_one + total_two, memory, normer, joined)


def local_step(state_carry, inputs):
    memory, normer, running = state_carry
    query_block, key_block, value_block, input_block, forget_block = inputs
    length = query_block.shape[0]
    highest = lax.Precision.HIGHEST
    query_scale = query_block.shape[2] ** (-0.5)
    causal = jnp.tril(jnp.ones((length, length), dtype=bool))[:, :, None]
    cumulative = jnp.cumsum(forget_block, axis=0)
    logits = cumulative[:, None, :] - cumulative[None, :, :] + input_block[None, :, :]
    logits = jnp.where(causal, logits, -jnp.inf)
    carried = cumulative + running[None, :]
    stable = jnp.maximum(carried, jnp.max(logits, axis=1))
    carry_weight = jnp.exp(carried - stable)
    raw = (
        jnp.einsum("thd,shd->tsh", query_block, key_block, preferred_element_type=jnp.float32)
        * query_scale
    )
    scores = raw * jnp.exp(logits - stable[:, None, :])
    scaled_query = query_block.astype(jnp.float32) * query_scale
    numerator = carry_weight[:, :, None] * jnp.einsum(
        "hvd,thd->thv", memory, scaled_query, precision=highest
    )
    numerator = numerator + jnp.einsum(
        "tsh,shv->thv", scores.astype(jnp.bfloat16), value_block, preferred_element_type=jnp.float32
    )
    denominator = carry_weight * jnp.einsum(
        "hd,thd->th", normer, scaled_query, precision=highest
    ) + jnp.sum(scores, axis=1)
    last_sum = cumulative[-1]
    weights_log = last_sum[None, :] - cumulative + input_block
    new_running = jnp.maximum(last_sum + running, jnp.max(weights_log, axis=0))
    decay_factor = jnp.exp(last_sum + running - new_running)
    weighted = (
        key_block.astype(jnp.float32) * jnp.exp(weights_log - new_running[None, :])[:, :, None]
    )
    memory = decay_factor[:, None, None] * memory + jnp.einsum(
        "shv,shd->hvd",
        value_block,
        weighted.astype(jnp.bfloat16),
        preferred_element_type=jnp.float32,
    )
    normer = decay_factor[:, None] * normer + jnp.sum(weighted, axis=0)
    return ((memory, normer, new_running), (numerator, denominator, stable))


def local(
    residual_entry_input,
    query_matrix_rows,
    key_matrix_rows,
    value_matrix_rows,
    output_gate_logits,
    input_gate_logits,
    forget_gate_logits,
    forget_decay_offset,
    head_norm_gain,
    cell_output_weight,
    feedforward_norm_gain,
    gate_up_weight,
    value_up_weight,
    gate_filter_taps,
    value_filter_taps,
    down_projection_weight,
):
    highest = lax.Precision.HIGHEST
    token_count = query_matrix_rows.shape[0]
    head_count = input_gate_logits.shape[1]
    key_width = query_matrix_rows.shape[1] // head_count
    value_width = value_matrix_rows.shape[1] // head_count
    query_scale = key_width ** (-0.5)
    queries_low = query_matrix_rows.reshape(token_count, head_count, key_width)
    keys_low = key_matrix_rows.reshape(token_count, head_count, key_width)
    values_low = value_matrix_rows.reshape(token_count, head_count, value_width)
    input_log_value, forget_log_sigmoid = gate_log_values(
        input_gate_logits, forget_gate_logits, forget_decay_offset
    )
    cumulative = jnp.cumsum(forget_log_sigmoid, axis=0)
    total_log = cumulative[-1]
    block_count = token_count // BLOCK

    def blocks(tensor):
        return tensor.reshape((block_count, BLOCK) + tensor.shape[1:])

    initial = (
        jnp.zeros((head_count, value_width, key_width), jnp.float32),
        jnp.zeros((head_count, key_width), jnp.float32),
        jnp.full((head_count,), neg_large, jnp.float32),
    )
    end_state, (numerator, denominator, stable) = lax.scan(
        local_step,
        initial,
        (
            blocks(queries_low),
            blocks(keys_low),
            blocks(values_low),
            blocks(input_log_value),
            blocks(forget_log_sigmoid),
        ),
    )
    end_memory, end_normer, end_running = end_state
    identity = (
        jnp.zeros((head_count,), jnp.float32),
        jnp.zeros((head_count, value_width, key_width), jnp.float32),
        jnp.zeros((head_count, key_width), jnp.float32),
        jnp.full((head_count,), neg_large, jnp.float32),
    )
    prefix = carried_in(
        (total_log, end_memory, end_normer, end_running), "sp", combine_states, identity
    )
    numerator = numerator.reshape(token_count, head_count, value_width)
    denominator = denominator.reshape(token_count, head_count)
    stable = stable.reshape(token_count, head_count)
    _, prior_memory, prior_normer, prior_running = prefix
    scaled_query = queries_low.astype(jnp.float32) * query_scale
    prior_log = cumulative + prior_running[None, :]
    top_log = jnp.maximum(stable, prior_log)
    local_weight = jnp.exp(stable - top_log)
    prior_weight = jnp.exp(prior_log - top_log)
    numerator = local_weight[:, :, None] * numerator + prior_weight[:, :, None] * jnp.einsum(
        "hvd,thd->thv", prior_memory, scaled_query, precision=highest
    )
    denominator = local_weight * denominator + prior_weight * jnp.einsum(
        "hd,thd->th", prior_normer, scaled_query, precision=highest
    )
    memory_out = numerator / jnp.maximum(jnp.abs(denominator), jnp.exp(-top_log))[:, :, None]
    normed = (
        memory_out
        * lax.rsqrt(jnp.mean(memory_out * memory_out, axis=-1, keepdims=True) + eps)
        * head_norm_gain[None, :, :]
    )
    gated_rows = (
        normed.reshape(token_count, head_count * value_width)
        * jax.nn.sigmoid(output_gate_logits.astype(jnp.float32))
    ).astype(jnp.bfloat16)
    whole_out = lax.all_gather(cell_output_weight, "tp", axis=0, tiled=True)
    own_rows = lax.all_to_all(gated_rows, "tp", split_axis=0, concat_axis=1, tiled=True)
    mixed_rows = jnp.dot(own_rows, whole_out, preferred_element_type=jnp.float32)
    stream_wide = residual_entry_input.astype(jnp.float32) + mixed_rows
    stream = stream_wide.astype(jnp.bfloat16)
    stream_wide = lax.optimization_barrier(stream).astype(jnp.float32)
    normed_rows = (
        stream_wide
        * lax.rsqrt(jnp.mean(stream_wide * stream_wide, axis=-1, keepdims=True) + eps)
        * feedforward_norm_gain[None, :]
    ).astype(jnp.bfloat16)
    group_rows = lax.all_gather(normed_rows, "tp", axis=0, tiled=True)
    earlier_rows = shifted(group_rows[-2:], "sp", 1)
    window = jnp.concatenate([earlier_rows, group_rows], axis=0)
    up_gate = jnp.dot(
        window,
        lax.all_gather(gate_up_weight, "sp", axis=0, tiled=True),
        preferred_element_type=jnp.float32,
    )
    up_value = jnp.dot(
        window,
        lax.all_gather(value_up_weight, "sp", axis=0, tiled=True),
        preferred_element_type=jnp.float32,
    )
    conv_g = (
        gate_filter_taps[0][None, :] * up_gate[:-2]
        + gate_filter_taps[1][None, :] * up_gate[1:-1]
        + gate_filter_taps[2][None, :] * up_gate[2:]
    )
    conv_v = (
        value_filter_taps[0][None, :] * up_value[:-2]
        + value_filter_taps[1][None, :] * up_value[1:-1]
        + value_filter_taps[2][None, :] * up_value[2:]
    )
    hidden = (jax.nn.silu(conv_g) * conv_v).astype(jnp.bfloat16)
    whole_down = lax.all_gather(down_projection_weight, "sp", axis=1, tiled=True)
    ffn_rows = lax.psum_scatter(
        jnp.dot(hidden, whole_down, preferred_element_type=jnp.float32).astype(jnp.bfloat16),
        "tp",
        scatter_dimension=0,
        tiled=True,
    ).astype(jnp.float32)
    return (stream_wide + ffn_rows).astype(jnp.bfloat16)


def solution(mesh):
    in_specs = (
        P(("sp", "tp"), None),
        P("sp", "tp"),
        P("sp", "tp"),
        P("sp", "tp"),
        P("sp", "tp"),
        P("sp", "tp"),
        P("sp", "tp"),
        P("sp", "tp"),
        P("tp", None),
        P("tp", None),
        P(),
        P("sp", "tp"),
        P("sp", "tp"),
        P(None, "tp"),
        P(None, "tp"),
        P("tp", "sp"),
    )
    out_specs = P(("sp", "tp"), None)
    return jax.shard_map(local, mesh=mesh, in_specs=in_specs, out_specs=out_specs, check_vma=False)
```

profile of v0, /device:TPU:0, one launch (start us, length us, event | category | flops | bytes accessed | tf_op | source)
XLA Modules:
  0.0 629.0 jit_solution(18224603662122398015)
XLA Ops:
  7.6 1.3 reshape.215
  9.9 2.0 reshape.216
  12.8 105.2 %while.39 = (s32[]{:T(128)}, f32[2,256,128]{2,1,0:T(8,128)S(1)}, f32[2,128]{1,0:T(2,128)S(1)}, f32[2]{0:T(128)S(1)}, f32[8,128,2,256]{1,0,3,2:T(8,128)}, /*index...) while((s32[]{:T(128)}, f32[2,256,128]{2,1,0:T(8,128)S(1)}, ...), condition=%wide.region_6.7_spmd.clone, body=%wide.region_0.6_spmd.clone.sunk | while | flops 144166400 | bytes 4685610 | solution.py:144
  17.3 8.2 %dynamic_update_slice.19 = f32[8,128,2,256]{1,0,3,2:T(8,128)} dynamic-update-slice(f32[8,128,2,256]{1,0,3,2:T(8,128)} %get-tuple-element.661, f32[1,128,2,256]{1,0,3,2:T(1,128)S(1)} %copy.248, s32[]{:T(128)} %get-tuple-element.657, s32[]{:T(128)} %constant.83.clone.1..sunk, s32[]{:T(128)} %constant.83.clone.1..sunk, s32[]{:T(128)} %constant.83.clone.1..sunk) | dynamic-update-slice | bytes 524292 | tf_op jit(solution)/shard_map/while/body/jit(dynamic_update_index_in_dim)/dynamic_update_slice | solution.py:144
  30.5 8.2 %dynamic_update_slice.19 = f32[8,128,2,256]{1,0,3,2:T(8,128)} dynamic-update-slice(f32[8,128,2,256]{1,0,3,2:T(8,128)} %get-tuple-element.661, f32[1,128,2,256]{1,0,3,2:T(1,128)S(1)} %copy.248, s32[]{:T(128)} %get-tuple-element.657, s32[]{:T(128)} %constant.83.clone.1..sunk, s32[]{:T(128)} %constant.83.clone.1..sunk, s32[]{:T(128)} %constant.83.clone.1..sunk) | dynamic-update-slice | bytes 524292 | tf_op jit(solution)/shard_map/while/body/jit(dynamic_update_index_in_dim)/dynamic_update_slice | solution.py:144
  43.7 8.2 %dynamic_update_slice.19 = f32[8,128,2,256]{1,0,3,2:T(8,128)} dynamic-update-slice(f32[8,128,2,256]{1,0,3,2:T(8,128)} %get-tuple-element.661, f32[1,128,2,256]{1,0,3,2:T(1,128)S(1)} %copy.248, s32[]{:T(128)} %get-tuple-element.657, s32[]{:T(128)} %constant.83.clone.1..sunk, s32[]{:T(128)} %constant.83.clone.1..sunk, s32[]{:T(128)} %constant.83.clone.1..sunk) | dynamic-update-slice | bytes 524292 | tf_op jit(solution)/shard_map/while/body/jit(dynamic_update_index_in_dim)/dynamic_update_slice | solution.py:144
  56.8 8.2 %dynamic_update_slice.19 = f32[8,128,2,256]{1,0,3,2:T(8,128)} dynamic-update-slice(f32[8,128,2,256]{1,0,3,2:T(8,128)} %get-tuple-element.661, f32[1,128,2,256]{1,0,3,2:T(1,128)S(1)} %copy.248, s32[]{:T(128)} %get-tuple-element.657, s32[]{:T(128)} %constant.83.clone.1..sunk, s32[]{:T(128)} %constant.83.clone.1..sunk, s32[]{:T(128)} %constant.83.clone.1..sunk) | dynamic-update-slice | bytes 524292 | tf_op jit(solution)/shard_map/while/body/jit(dynamic_update_index_in_dim)/dynamic_update_slice | solution.py:144
  70.0 8.2 %dynamic_update_slice.19 = f32[8,128,2,256]{1,0,3,2:T(8,128)} dynamic-update-slice(f32[8,128,2,256]{1,0,3,2:T(8,128)} %get-tuple-element.661, f32[1,128,2,256]{1,0,3,2:T(1,128)S(1)} %copy.248, s32[]{:T(128)} %get-tuple-element.657, s32[]{:T(128)} %constant.83.clone.1..sunk, s32[]{:T(128)} %constant.83.clone.1..sunk, s32[]{:T(128)} %constant.83.clone.1..sunk) | dynamic-update-slice | bytes 524292 | tf_op jit(solution)/shard_map/while/body/jit(dynamic_update_index_in_dim)/dynamic_update_slice | solution.py:144
  83.1 8.2 %dynamic_update_slice.19 = f32[8,128,2,256]{1,0,3,2:T(8,128)} dynamic-update-slice(f32[8,128,2,256]{1,0,3,2:T(8,128)} %get-tuple-element.661, f32[1,128,2,256]{1,0,3,2:T(1,128)S(1)} %copy.248, s32[]{:T(128)} %get-tuple-element.657, s32[]{:T(128)} %constant.83.clone.1..sunk, s32[]{:T(128)} %constant.83.clone.1..sunk, s32[]{:T(128)} %constant.83.clone.1..sunk) | dynamic-update-slice | bytes 524292 | tf_op jit(solution)/shard_map/while/body/jit(dynamic_update_index_in_dim)/dynamic_update_slice | solution.py:144
  96.3 8.2 %dynamic_update_slice.19 = f32[8,128,2,256]{1,0,3,2:T(8,128)} dynamic-update-slice(f32[8,128,2,256]{1,0,3,2:T(8,128)} %get-tuple-element.661, f32[1,128,2,256]{1,0,3,2:T(1,128)S(1)} %copy.248, s32[]{:T(128)} %get-tuple-element.657, s32[]{:T(128)} %constant.83.clone.1..sunk, s32[]{:T(128)} %constant.83.clone.1..sunk, s32[]{:T(128)} %constant.83.clone.1..sunk) | dynamic-update-slice | bytes 524292 | tf_op jit(solution)/shard_map/while/body/jit(dynamic_update_index_in_dim)/dynamic_update_slice | solution.py:144
  109.4 8.2 %dynamic_update_slice.19 = f32[8,128,2,256]{1,0,3,2:T(8,128)} dynamic-update-slice(f32[8,128,2,256]{1,0,3,2:T(8,128)} %get-tuple-element.661, f32[1,128,2,256]{1,0,3,2:T(1,128)S(1)} %copy.248, s32[]{:T(128)} %get-tuple-element.657, s32[]{:T(128)} %constant.83.clone.1..sunk, s32[]{:T(128)} %constant.83.clone.1..sunk, s32[]{:T(128)} %constant.83.clone.1..sunk) | dynamic-update-slice | bytes 524292 | tf_op jit(solution)/shard_map/while/body/jit(dynamic_update_index_in_dim)/dynamic_update_slice | solution.py:144
  122.2 22.3 %all-gather.3 = bf16[8,1,2]{2,1,0:T(2,128)(2,1)S(1)} all-gather(bf16[1,1,2]{2,1,0:T(2,128)(2,1)S(1)} %bitcast.273), channel_id=1, replica_groups=mesh['sp'=8,'tp'=4] {'sp'}, dimensions={0}, use_global_device_ids=true | all-gather | bytes 36 | tf_op jit(solution)/shard_map/all_gather | solution.py:14
  144.5 17.5 %all-reduce = bf16[16]{0:T(256)(128)(2,1)S(1)} all-reduce(bf16[16]{0:T(256)(128)(2,1)S(1)} %dynamic-update-slice), channel_id=2, replica_groups=mesh['sp'=8,'tp'=4] {'sp'}, use_global_device_ids=true, to_apply=%add | all-reduce | flops 16 | bytes 64
  163.5 1.3 copy.156
  164.8 1.7 reshape.187
  166.5 18.0 %all-gather.4 = bf16[8,2,128]{2,1,0:T(2,128)(2,1)S(1)} all-gather(bf16[1,2,128]{2,1,0:T(2,128)(2,1)S(1)} %convert_bitcast_fusion), channel_id=4, replica_groups=mesh['sp'=8,'tp'=4] {'sp'}, dimensions={0}, use_global_device_ids=true | all-gather | bytes 4608 | tf_op jit(solution)/shard_map/all_gather | solution.py:14
  184.5 10.5 %while.40 = (s32[]{:T(128)}, f32[2,256,128]{2,1,0:T(8,128)S(1)}, f32[2,128]{1,0:T(2,128)S(1)}, f32[2]{0:T(128)S(1)}, s32[]{:T(128)}, /*index=5*/bf16[8,2]{0,1:T(...) while((s32[]{:T(128)}, f32[2,256,128]{2,1,0:T(8,128)S(1)}, ...), condition=%wide.region_10.11_spmd.clone, body=%wide.region_9.10_spmd.clone.sunk | while | flops 394772 | bytes 658157 | solution.py:29
  196.2 2.2 multiply_reduce_fusion
  198.7 1.9 copy.141
  200.6 2.5 multiply_convert_fusion
  203.1 26.9 %all_to_all.19 = bf16[4,256,512]{2,1,0:T(8,128)(2,1)S(1)} all-to-all(bf16[4,256,512]{2,1,0:T(8,128)(2,1)S(1)} %bitcast.262), channel_id=1, replica_groups=mesh['sp'=8,'tp'=4] {'tp'}, dimensions={0} | all-to-all | bytes 2097152 | tf_op jit(solution)/shard_map/all_to_all | solution.py:191
  230.5 5.7 fusion.45
  239.9 33.9 %all-gather.14.cloned.1.call-done = bf16[1024,2048]{1,0:T(8,128)(2,1)} async-done(((bf16[256,2048]{1,0:T(8,128)(2,1)}), bf16[1024,2048]{1,0:T(8,128)(2,1)}) %all-gather.14.cloned.1.call-update) | async-done | bytes 4194320 | tf_op jit(solution)/shard_map/all_gather | solution.py:201
  274.6 3.4 collective-permute-start
  278.1 90.1 %all-gather.16.cloned.1.call-done = bf16[2048,1408]{1,0:T(8,128)(2,1)} async-done(((bf16[256,1408]{1,0:T(8,128)(2,1)}), bf16[2048,1408]{1,0:T(8,128)(2,1)}) %all-gather.16.cloned.1.call-update) | async-done | bytes 5767184 | tf_op jit(solution)/shard_map/all_gather | solution.py:206
  368.2 11.9 %fusion.44 = f32[1026,1408]{1,0:T(8,128)} fusion(bf16[2048,1408]{1,0:T(8,128)(2,1)} %all-gather.16.cloned.1.call-done, bf16[1024,2048]{1,0:T(8,128)(2,1)} %all-gather.14.cloned.1.call-done, bf16[2,2048]{1,0:T(2,128)(2,1)S(1)} %collective-permute-done), kind=kOutput, calls=%fused_computation.90 | convolution fusion | flops 5925519360 | bytes 15748096 | tf_op jit(solution)/shard_map/dot_general | solution.py:204
  380.1 80.6 %all-gather.18.cloned.1.call-done = bf16[2048,1408]{1,0:T(8,128)(2,1)} async-done(((bf16[256,1408]{1,0:T(8,128)(2,1)}), bf16[2048,1408]{1,0:T(8,128)(2,1)}) %all-gather.18.cloned.1.call-update) | async-done | bytes 5767184 | tf_op jit(solution)/shard_map/all_gather | solution.py:211
  460.7 11.9 %fusion.43 = f32[1026,1408]{1,0:T(8,128)} fusion(bf16[2048,1408]{1,0:T(8,128)(2,1)} %all-gather.18.cloned.1.call-done, bf16[1024,2048]{1,0:T(8,128)(2,1)} %all-gather.14.cloned.1.call-done, bf16[2,2048]{1,0:T(2,128)(2,1)S(1)} %collective-permute-done), kind=kOutput, calls=%fused_computation.89 | convolution fusion | flops 5925519360 | bytes 15748096 | tf_op jit(solution)/shard_map/dot_general | solution.py:209
  472.6 81.3 %all-gather.20.cloned.1.call-done = bf16[1408,2048]{1,0:T(8,128)(2,1)} async-done(((bf16[1408,256]{1,0:T(8,128)(2,1)}), bf16[1408,2048]{1,0:T(8,128)(2,1)}) %all-gather.20.cloned.1.call-update) | async-done | bytes 5767184 | tf_op jit(solution)/shard_map/all_gather | solution.py:225
  554.0 22.7 %convolution_convert_fusion = bf16[1024,2048]{1,0:T(8,128)(2,1)} fusion(bf16[1408,2048]{1,0:T(8,128)(2,1)} %all-gather.20.cloned.1.call-done, f32[1026,1408]{1,0:T(8,128)} %fusion.43, f32[1026,1408]{1,0:T(8,128)} %fusion.44, f32[1408]{0:T(1024)S(1)} %get-tuple-element.403, f32[1408]{0:T(1024)S(1)} %get-tuple-element.404, f32[1408]{0:T(1024)S(1)} %get-tuple-element.402, ...), kind=kOutput, calls=%fused_computation.85 | convolution fusion | flops 5930745856 | bytes 44598272 | tf_op jit(solution)/shard_map/dot_general | solution.py:227
  576.7 42.9 %reduce-scatter.2.cloned.1.call-done = bf16[256,2048]{1,0:T(8,128)(2,1)} async-done(((bf16[1024,2048]{1,0:T(8,128)(2,1)}), bf16[256,2048]{1,0:T(8,128)(2,1)}) %reduce-scatter.2.cloned.1.call-update) | async-done | bytes 1048592 | tf_op jit(solution)/shard_map/reduce_scatter | solution.py:226
  619.6 2.6 fusion.49
  (337 shorter events, 63.3 us)
Async XLA Ops:
  6.5 5.3 copy-start.1
  6.5 178.0 %all-gather.22.cloned.1.call-start = ((), (), s32[]{:S(2)}) async-start(), calls=%async_computation.8 | async-start | bytes 1179648 | tf_op jit(solution)/shard_map/all_gather | solution.py:14
  12.8 107.7 %copy-start.7 = (u32[32]{0:T(128)S(1)}, u32[32]{0:T(128)}, u32[]{:S(2)}) copy-start(u32[32]{0:T(128)} %constant.101) | copy-start | bytes 388
  118.7 111.8 %all-gather.12.cloned.1.call-start = ((), (), s32[]{:S(2)}) async-start(), calls=%async_computation.2 | async-start | bytes 10485760 | tf_op jit(solution)/shard_map/all_gather | solution.py:190
  119.4 154.4 %all-gather.14.cloned.1.call-start = ((), (), s32[]{:S(2)}) async-start(), calls=%async_computation.3 | async-start | bytes 5242880 | tf_op jit(solution)/shard_map/all_gather | solution.py:201
  163.5 31.6 %copy-start.2 = (bf16[1024,256]{1,0:T(8,128)(2,1)S(1)}, bf16[1024,256]{1,0:T(8,128)(2,1)}, u32[]{:S(2)}) copy-start(bf16[1024,256]{1,0:T(8,128)(2,1)} %param.21) | copy-start | bytes 1572868
  196.2 2.3 copy-start.6
  200.6 29.9 %copy-start = (bf16[256,2048]{1,0:T(8,128)(2,1)S(1)}, bf16[256,2048]{1,0:T(8,128)(2,1)}, u32[]{:S(2)}) copy-start(bf16[256,2048]{1,0:T(8,128)(2,1)} %param.20) | copy-start | bytes 3145732
  230.5 6.1 copy-start.5
  236.3 41.7 %copy-start.3 = (f32[3,1408]{1,0:T(4,128)S(1)}, f32[3,1408]{1,0:T(4,128)}, u32[]{:S(2)}) copy-start(f32[3,1408]{1,0:T(4,128)} %param.34) | copy-start | bytes 50692
  236.3 41.7 %copy-start.4 = (f32[3,1408]{1,0:T(4,128)S(1)}, f32[3,1408]{1,0:T(4,128)}, u32[]{:S(2)}) copy-start(f32[3,1408]{1,0:T(4,128)} %param.33) | copy-start | bytes 50692
  237.9 130.3 %all-gather.16.cloned.1.call-start = ((), (), s32[]{:S(2)}) async-start(), calls=%async_computation.4 | async-start | bytes 6488064 | tf_op jit(solution)/shard_map/all_gather | solution.py:206
  238.5 222.3 %all-gather.18.cloned.1.call-start = ((), (), s32[]{:S(2)}) async-start(), calls=%async_computation.5 | async-start | bytes 6488064 | tf_op jit(solution)/shard_map/all_gather | solution.py:211
  239.1 314.9 %all-gather.20.cloned.1.call-start = ((), (), s32[]{:S(2)}) async-start(), calls=%async_computation.6 | async-start | bytes 6488064 | tf_op jit(solution)/shard_map/all_gather | solution.py:225
  239.7 379.9 %reduce-scatter.2.cloned.1.call-start = ((), (), s32[]{:S(2)}) async-start(), calls=%async_computation.7 | async-start | bytes 5242880 | tf_op jit(solution)/shard_map/reduce_scatter | solution.py:226
  274.6 93.6 %collective-permute-start = (bf16[2,2048]{1,0:T(2,128)(2,1)S(1)}, bf16[2,2048]{1,0:T(2,128)(2,1)S(1)}, u32[]{:S(2)}, u32[]{:S(2)}) collective-permute-start(bf16[2,2048]{1,0:T(2,128)(2,1)S(1)} %slice.72), channel_id=1, source_target_pairs={{0,4},{4,8},{8,12},{12,16},{16,20},{20,24},{24,28},{1,5},{5,9},{9,... | collective-permute-start | bytes 24584 | tf_op jit(solution)/shard_map/ppermute | solution.py:35
Sparse Core Ops, SparseCore 0:
  118.8 43.2 all-gather.21
  163.6 66.6 all-gather.11
  238.0 35.7 all-gather.13
  275.8 92.3 all-gather.15
  370.2 90.4 all-gather.17
  462.6 91.2 all-gather.19
  576.8 42.7 reduce-scatter.1
where the time goes:
time: 631 us; the launch traced here: 629 us
  waiting for transfers between devices  331 us (52%)
  local copies, waits for them, and re-layouts  97.1 us (15%)
  blocking collectives  84.7 us (13%)
  matrix products  67.5 us (11%)
  other arithmetic  29.4 us (5%)
  between operations  14.4 us (2%)
    all_gather x1, waiting for transfers between devices, local(): lax.all_gather(gate_up_weight, 'sp', axis=0, tiled=True)  90.1 us
    all_gather x1, waiting for transfers between devices, local(): lax.all_gather(down_projection_weight, 'sp', axis=1, tiled=True)  81.3 us
    all_gather x1, waiting for transfers between devices, local(): lax.all_gather(value_up_weight, 'sp', axis=0, tiled=True)  80.6 us
    dynamic_update_slice x16, local copies, waits for them, and re-layouts, local(): lax.scan(local_step, initial, (blocks(queries_low), blocks(keys_low), blo...  66.7 us
    reduce_scatter x1, waiting for transfers between devices, local(): lax.psum_scatter(jnp.dot(hidden, whole_down, preferred_element_type=jnp.f...  42.9 us
    all_gather x2, blocking collectives, carried_in(): lax.all_gather(part.astype(kind), axis)  40.3 us
    all_gather x1, waiting for transfers between devices, local(): group_rows = lax.all_gather(normed_rows, 'tp', axis=0, tiled=True)  33.9 us
    all_to_all x1, blocking collectives, local(): lax.all_to_all(gated_rows, 'tp', split_axis=0, concat_axis=1, tiled=True)  26.9 us
  transfers between devices with their start and end apart: 8, of which 5 were waited for; matrix products, arithmetic and copies ran while one was open for 8% of the time, Pallas kernels for 0%

commit v1 on v0

--- a/solution.py
+++ b/solution.py
@@ -198,7 +198,12 @@
         * lax.rsqrt(jnp.mean(stream_wide * stream_wide, axis=-1, keepdims=True) + eps)
         * feedforward_norm_gain[None, :]
     ).astype(jnp.bfloat16)
-    group_rows = lax.all_gather(normed_rows, "tp", axis=0, tiled=True)
+    ring = [normed_rows]
+    for hop in range(3):
+        ring.append(lax.ppermute(ring[-1], "tp", [(dev, (dev + 1) % 4) for dev in range(4)]))
+    group_rows = jnp.roll(
+        jnp.concatenate(ring[::-1], axis=0), (lax.axis_index("tp") + 1) * ring[0].shape[0], axis=0
+    )
     earlier_rows = shifted(group_rows[-2:], "sp", 1)
     window = jnp.concatenate([earlier_rows, group_rows], axis=0)
     up_gate = jnp.dot(

time: 631 us -> 591 us (0.937)
  waiting for transfers between devices: 331 us -> 286 us
    all_gather x1, waiting for transfers between devices: 90.1 us -> 36.5 us  [local(): lax.all_gather(gate_up_weight, 'sp', axis=0, tiled=True)]
    ppermute x0 -> x3, waiting for transfers between devices: none -> 42.4 us  [local(): lax.ppermute(ring[-1], 'tp', [(dev, (dev + 1) % 4) for dev in range(4)])]
    all_gather x1 -> x0, waiting for transfers between devices: 33.9 us -> none  [local(): group_rows = lax.all_gather(normed_rows, 'tp', axis=0, tiled=True)]
  transfers between devices with their start and end apart: 8 -> 10, of which waited for: 5 -> 7; matrix products, arithmetic and copies ran while one was open for 8% -> 11% of each run, Pallas kernels for 0% -> 0%
where the time goes in v1:
time: 591 us; the launch traced here: 588 us
  waiting for transfers between devices  286 us (48%)
  local copies, waits for them, and re-layouts  103 us (17%)
  blocking collectives  83.4 us (14%)
  matrix products  67.5 us (11%)
  other arithmetic  29 us (5%)
  between operations  14.4 us (2%)
    all_gather x1, waiting for transfers between devices, local(): lax.all_gather(down_projection_weight, 'sp', axis=1, tiled=True)  81.3 us
    all_gather x1, waiting for transfers between devices, local(): lax.all_gather(value_up_weight, 'sp', axis=0, tiled=True)  80.7 us
    dynamic_update_slice x16, local copies, waits for them, and re-layouts, local(): lax.scan(local_step, initial, (blocks(queries_low), blocks(keys_low), blo...  66.7 us
    reduce_scatter x1, waiting for transfers between devices, local(): lax.psum_scatter(jnp.dot(hidden, whole_down, preferred_element_type=jnp.f...  42.9 us
    ppermute x3, waiting for transfers between devices, local(): lax.ppermute(ring[-1], 'tp', [(dev, (dev + 1) % 4) for dev in range(4)])  42.4 us
    all_gather x1, waiting for transfers between devices, local(): lax.all_gather(gate_up_weight, 'sp', axis=0, tiled=True)  36.5 us
    all_gather x2, blocking collectives, carried_in(): lax.all_gather(part.astype(kind), axis)  34.6 us
    all_to_all x1, blocking collectives, local(): lax.all_to_all(gated_rows, 'tp', split_axis=0, concat_axis=1, tiled=True)  25.5 us
  transfers between devices with their start and end apart: 10, of which 7 were waited for; matrix products, arithmetic and copies ran while one was open for 11% of the time, Pallas kernels for 0%

profile of v1, /device:TPU:0, one launch (start us, length us, event | category | flops | bytes accessed | tf_op | source)
XLA Modules:
  0.0 588.2 jit_solution(12758611576676642751)
XLA Ops:
  9.8 2.0 reshape.216
  11.8 2.0 reshape.217
  13.8 105.2 %while.39 = (s32[]{:T(128)}, f32[2,256,128]{2,1,0:T(8,128)S(1)}, f32[2,128]{1,0:T(2,128)S(1)}, f32[2]{0:T(128)S(1)}, f32[8,128,2,256]{1,0,3,2:T(8,128)}, /*index...) while((s32[]{:T(128)}, f32[2,256,128]{2,1,0:T(8,128)S(1)}, ...), condition=%wide.region_6.7_spmd.clone, body=%wide.region_0.6_spmd.clone.sunk | while | flops 144166400 | bytes 4685610 | solution.py:144
  18.3 8.2 %dynamic_update_slice.19 = f32[8,128,2,256]{1,0,3,2:T(8,128)} dynamic-update-slice(f32[8,128,2,256]{1,0,3,2:T(8,128)} %get-tuple-element.661, f32[1,128,2,256]{1,0,3,2:T(1,128)S(1)} %copy.248, s32[]{:T(128)} %get-tuple-element.657, s32[]{:T(128)} %constant.105.clone.1..sunk, s32[]{:T(128)} %constant.105.clone.1..sunk, s32[]{:T(128)} %constant.105.clone.1..sunk) | dynamic-update-slice | bytes 524292 | tf_op jit(solution)/shard_map/while/body/jit(dynamic_update_index_in_dim)/dynamic_update_slice | solution.py:144
  31.5 8.2 %dynamic_update_slice.19 = f32[8,128,2,256]{1,0,3,2:T(8,128)} dynamic-update-slice(f32[8,128,2,256]{1,0,3,2:T(8,128)} %get-tuple-element.661, f32[1,128,2,256]{1,0,3,2:T(1,128)S(1)} %copy.248, s32[]{:T(128)} %get-tuple-element.657, s32[]{:T(128)} %constant.105.clone.1..sunk, s32[]{:T(128)} %constant.105.clone.1..sunk, s32[]{:T(128)} %constant.105.clone.1..sunk) | dynamic-update-slice | bytes 524292 | tf_op jit(solution)/shard_map/while/body/jit(dynamic_update_index_in_dim)/dynamic_update_slice | solution.py:144
  44.6 8.2 %dynamic_update_slice.19 = f32[8,128,2,256]{1,0,3,2:T(8,128)} dynamic-update-slice(f32[8,128,2,256]{1,0,3,2:T(8,128)} %get-tuple-element.661, f32[1,128,2,256]{1,0,3,2:T(1,128)S(1)} %copy.248, s32[]{:T(128)} %get-tuple-element.657, s32[]{:T(128)} %constant.105.clone.1..sunk, s32[]{:T(128)} %constant.105.clone.1..sunk, s32[]{:T(128)} %constant.105.clone.1..sunk) | dynamic-update-slice | bytes 524292 | tf_op jit(solution)/shard_map/while/body/jit(dynamic_update_index_in_dim)/dynamic_update_slice | solution.py:144
  57.8 8.2 %dynamic_update_slice.19 = f32[8,128,2,256]{1,0,3,2:T(8,128)} dynamic-update-slice(f32[8,128,2,256]{1,0,3,2:T(8,128)} %get-tuple-element.661, f32[1,128,2,256]{1,0,3,2:T(1,128)S(1)} %copy.248, s32[]{:T(128)} %get-tuple-element.657, s32[]{:T(128)} %constant.105.clone.1..sunk, s32[]{:T(128)} %constant.105.clone.1..sunk, s32[]{:T(128)} %constant.105.clone.1..sunk) | dynamic-update-slice | bytes 524292 | tf_op jit(solution)/shard_map/while/body/jit(dynamic_update_index_in_dim)/dynamic_update_slice | solution.py:144
  70.9 8.2 %dynamic_update_slice.19 = f32[8,128,2,256]{1,0,3,2:T(8,128)} dynamic-update-slice(f32[8,128,2,256]{1,0,3,2:T(8,128)} %get-tuple-element.661, f32[1,128,2,256]{1,0,3,2:T(1,128)S(1)} %copy.248, s32[]{:T(128)} %get-tuple-element.657, s32[]{:T(128)} %constant.105.clone.1..sunk, s32[]{:T(128)} %constant.105.clone.1..sunk, s32[]{:T(128)} %constant.105.clone.1..sunk) | dynamic-update-slice | bytes 524292 | tf_op jit(solution)/shard_map/while/body/jit(dynamic_update_index_in_dim)/dynamic_update_slice | solution.py:144
  84.1 8.2 %dynamic_update_slice.19 = f32[8,128,2,256]{1,0,3,2:T(8,128)} dynamic-update-slice(f32[8,128,2,256]{1,0,3,2:T(8,128)} %get-tuple-element.661, f32[1,128,2,256]{1,0,3,2:T(1,128)S(1)} %copy.248, s32[]{:T(128)} %get-tuple-element.657, s32[]{:T(128)} %constant.105.clone.1..sunk, s32[]{:T(128)} %constant.105.clone.1..sunk, s32[]{:T(128)} %constant.105.clone.1..sunk) | dynamic-update-slice | bytes 524292 | tf_op jit(solution)/shard_map/while/body/jit(dynamic_update_index_in_dim)/dynamic_update_slice | solution.py:144
  97.2 8.2 %dynamic_update_slice.19 = f32[8,128,2,256]{1,0,3,2:T(8,128)} dynamic-update-slice(f32[8,128,2,256]{1,0,3,2:T(8,128)} %get-tuple-element.661, f32[1,128,2,256]{1,0,3,2:T(1,128)S(1)} %copy.248, s32[]{:T(128)} %get-tuple-element.657, s32[]{:T(128)} %constant.105.clone.1..sunk, s32[]{:T(128)} %constant.105.clone.1..sunk, s32[]{:T(128)} %constant.105.clone.1..sunk) | dynamic-update-slice | bytes 524292 | tf_op jit(solution)/shard_map/while/body/jit(dynamic_update_index_in_dim)/dynamic_update_slice | solution.py:144
  110.4 8.2 %dynamic_update_slice.19 = f32[8,128,2,256]{1,0,3,2:T(8,128)} dynamic-update-slice(f32[8,128,2,256]{1,0,3,2:T(8,128)} %get-tuple-element.661, f32[1,128,2,256]{1,0,3,2:T(1,128)S(1)} %copy.248, s32[]{:T(128)} %get-tuple-element.657, s32[]{:T(128)} %constant.105.clone.1..sunk, s32[]{:T(128)} %constant.105.clone.1..sunk, s32[]{:T(128)} %constant.105.clone.1..sunk) | dynamic-update-slice | bytes 524292 | tf_op jit(solution)/shard_map/while/body/jit(dynamic_update_index_in_dim)/dynamic_update_slice | solution.py:144
  123.3 23.3 %all-reduce = bf16[16]{0:T(256)(128)(2,1)S(1)} all-reduce(bf16[16]{0:T(256)(128)(2,1)S(1)} %dynamic-update-slice), channel_id=2, replica_groups=mesh['sp'=8,'tp'=4] {'sp'}, use_global_device_ids=true, to_apply=%add | all-reduce | flops 16 | bytes 64
  146.7 16.4 %all-gather.4 = bf16[8,2,128]{2,1,0:T(2,128)(2,1)S(1)} all-gather(bf16[1,2,128]{2,1,0:T(2,128)(2,1)S(1)} %convert_bitcast_fusion), channel_id=4, replica_groups=mesh['sp'=8,'tp'=4] {'sp'}, dimensions={0}, use_global_device_ids=true | all-gather | bytes 4608 | tf_op jit(solution)/shard_map/all_gather | solution.py:14
  164.3 18.2 %all-gather.3 = bf16[8,1,2]{2,1,0:T(2,128)(2,1)S(1)} all-gather(bf16[1,1,2]{2,1,0:T(2,128)(2,1)S(1)} %bitcast.275), channel_id=1, replica_groups=mesh['sp'=8,'tp'=4] {'sp'}, dimensions={0}, use_global_device_ids=true | all-gather | bytes 36 | tf_op jit(solution)/shard_map/all_gather | solution.py:14
  186.9 10.5 %while.40 = (s32[]{:T(128)}, f32[2,256,128]{2,1,0:T(8,128)S(1)}, f32[2,128]{1,0:T(2,128)S(1)}, f32[2]{0:T(128)S(1)}, s32[]{:T(128)}, /*index=5*/bf16[8,2]{0,1:T(...) while((s32[]{:T(128)}, f32[2,256,128]{2,1,0:T(8,128)S(1)}, ...), condition=%wide.region_10.11_spmd.clone, body=%wide.region_9.10_spmd.clone.sunk | while | flops 394772 | bytes 658157 | solution.py:29
  198.5 2.2 multiply_reduce_fusion
  202.9 2.5 multiply_convert_fusion
  205.5 25.5 %all_to_all.19 = bf16[4,256,512]{2,1,0:T(8,128)(2,1)S(1)} all-to-all(bf16[4,256,512]{2,1,0:T(8,128)(2,1)S(1)} %bitcast.262), channel_id=1, replica_groups=mesh['sp'=8,'tp'=4] {'tp'}, dimensions={0} | all-to-all | bytes 2097152 | tf_op jit(solution)/shard_map/all_to_all | solution.py:191
  231.5 5.7 fusion.45
  238.2 14.0 %collective-permute-done = bf16[256,2048]{1,0:T(8,128)(2,1)S(1)} collective-permute-done((bf16[256,2048]{1,0:T(8,128)(2,1)S(1)}, bf16[256,2048]{1,0:T(8,128)(2,1)S(1)}, u32[]{:S(2)}, u32[]{:S(2)}) %collective-permute-start) | collective-permute-done | bytes 1048608 | tf_op jit(solution)/shard_map/ppermute | solution.py:203
  252.1 14.2 %collective-permute-done.1 = bf16[256,2048]{1,0:T(8,128)(2,1)S(1)} collective-permute-done((bf16[256,2048]{1,0:T(8,128)(2,1)S(1)}, bf16[256,2048]{1,0:T(8,128)(2,1)S(1)}, u32[]{:S(2)}, u32[]{:S(2)}) %collective-permute-start.1) | collective-permute-done | bytes 1048608 | tf_op jit(solution)/shard_map/ppermute | solution.py:203
  266.5 14.2 %collective-permute-done.2 = bf16[256,2048]{1,0:T(8,128)(2,1)} collective-permute-done((bf16[256,2048]{1,0:T(8,128)(2,1)S(1)}, bf16[256,2048]{1,0:T(8,128)(2,1)}, u32[]{:S(2)}, u32[]{:S(2)}) %collective-permute-start.2) | collective-permute-done | bytes 1048608 | tf_op jit(solution)/shard_map/ppermute | solution.py:203
  284.3 3.4 collective-permute-start.3
  287.7 3.2 constant_dynamic-slice_fusion.7
  290.9 36.5 %all-gather.13.cloned.1.call-done = bf16[2048,1408]{1,0:T(8,128)(2,1)} async-done(((bf16[256,1408]{1,0:T(8,128)(2,1)}), bf16[2048,1408]{1,0:T(8,128)(2,1)}) %all-gather.13.cloned.1.call-update) | async-done | bytes 5767184 | tf_op jit(solution)/shard_map/all_gather | solution.py:211
  327.4 11.9 %fusion.44 = f32[1026,1408]{1,0:T(8,128)} fusion(bf16[2048,1408]{1,0:T(8,128)(2,1)} %all-gather.13.cloned.1.call-done, bf16[1024,2048]{1,0:T(8,128)(2,1)} %constant_dynamic-slice_fusion.7, bf16[2,2048]{1,0:T(2,128)(2,1)S(1)} %collective-permute-done.3), kind=kOutput, calls=%fused_computation.90 | convolution fusion | flops 5925519360 | bytes 15748096 | tf_op jit(solution)/shard_map/dot_general | solution.py:209
  339.3 80.7 %all-gather.15.cloned.1.call-done = bf16[2048,1408]{1,0:T(8,128)(2,1)} async-done(((bf16[256,1408]{1,0:T(8,128)(2,1)}), bf16[2048,1408]{1,0:T(8,128)(2,1)}) %all-gather.15.cloned.1.call-update) | async-done | bytes 5767184 | tf_op jit(solution)/shard_map/all_gather | solution.py:216
  420.0 11.9 %fusion.43 = f32[1026,1408]{1,0:T(8,128)} fusion(bf16[2048,1408]{1,0:T(8,128)(2,1)} %all-gather.15.cloned.1.call-done, bf16[1024,2048]{1,0:T(8,128)(2,1)} %constant_dynamic-slice_fusion.7, bf16[2,2048]{1,0:T(2,128)(2,1)S(1)} %collective-permute-done.3), kind=kOutput, calls=%fused_computation.89 | convolution fusion | flops 5925519360 | bytes 15748096 | tf_op jit(solution)/shard_map/dot_general | solution.py:214
  431.9 81.3 %all-gather.17.cloned.1.call-done = bf16[1408,2048]{1,0:T(8,128)(2,1)} async-done(((bf16[1408,256]{1,0:T(8,128)(2,1)}), bf16[1408,2048]{1,0:T(8,128)(2,1)}) %all-gather.17.cloned.1.call-update) | async-done | bytes 5767184 | tf_op jit(solution)/shard_map/all_gather | solution.py:230
  513.2 22.7 %convolution_convert_fusion = bf16[1024,2048]{1,0:T(8,128)(2,1)} fusion(bf16[1408,2048]{1,0:T(8,128)(2,1)} %all-gather.17.cloned.1.call-done, f32[1026,1408]{1,0:T(8,128)} %fusion.43, f32[1026,1408]{1,0:T(8,128)} %fusion.44, f32[1408]{0:T(1024)S(1)} %get-tuple-element.403, f32[1408]{0:T(1024)S(1)} %get-tuple-element.404, f32[1408]{0:T(1024)S(1)} %get-tuple-element.402, ...), kind=kOutput, calls=%fused_computation.85 | convolution fusion | flops 5930745856 | bytes 44598272 | tf_op jit(solution)/shard_map/dot_general | solution.py:232
  535.9 42.9 %reduce-scatter.2.cloned.1.call-done = bf16[256,2048]{1,0:T(8,128)(2,1)} async-done(((bf16[1024,2048]{1,0:T(8,128)(2,1)}), bf16[256,2048]{1,0:T(8,128)(2,1)}) %reduce-scatter.2.cloned.1.call-update) | async-done | bytes 1048592 | tf_op jit(solution)/shard_map/reduce_scatter | solution.py:231
  578.8 2.6 fusion.49
  (347 shorter events, 70.0 us)
Async XLA Ops:
  6.5 180.3 %all-gather.19.cloned.1.call-start = ((), (), s32[]{:S(2)}) async-start(), calls=%async_computation.7 | async-start | bytes 1179648 | tf_op jit(solution)/shard_map/all_gather | solution.py:14
  13.8 108.1 %copy-start.6 = (u32[32]{0:T(128)S(1)}, u32[32]{0:T(128)}, u32[]{:S(2)}) copy-start(u32[32]{0:T(128)} %constant.129) | copy-start | bytes 388
  119.7 77.7 %copy-start.1 = (bf16[1024,256]{1,0:T(8,128)(2,1)S(1)}, bf16[1024,256]{1,0:T(8,128)(2,1)}, u32[]{:S(2)}) copy-start(bf16[1024,256]{1,0:T(8,128)(2,1)} %param.21) | copy-start | bytes 1572868
  119.7 111.8 %all-gather.11.cloned.1.call-start = ((), (), s32[]{:S(2)}) async-start(), calls=%async_computation.2 | async-start | bytes 10485760 | tf_op jit(solution)/shard_map/all_gather | solution.py:190
  120.4 207.0 %all-gather.13.cloned.1.call-start = ((), (), s32[]{:S(2)}) async-start(), calls=%async_computation.3 | async-start | bytes 6488064 | tf_op jit(solution)/shard_map/all_gather | solution.py:211
  121.2 298.8 %all-gather.15.cloned.1.call-start = ((), (), s32[]{:S(2)}) async-start(), calls=%async_computation.4 | async-start | bytes 6488064 | tf_op jit(solution)/shard_map/all_gather | solution.py:216
  121.8 391.4 %all-gather.17.cloned.1.call-start = ((), (), s32[]{:S(2)}) async-start(), calls=%async_computation.5 | async-start | bytes 6488064 | tf_op jit(solution)/shard_map/all_gather | solution.py:230
  197.4 3.4 copy-start.5
  201.0 30.4 %copy-start = (bf16[256,2048]{1,0:T(8,128)(2,1)S(1)}, bf16[256,2048]{1,0:T(8,128)(2,1)}, u32[]{:S(2)}) copy-start(bf16[256,2048]{1,0:T(8,128)(2,1)} %param.20) | copy-start | bytes 3145732
  231.5 6.1 %copy-start.2 = (f32[2048]{0:T(1024)S(1)}, f32[2048]{0:T(1024)}, u32[]{:S(2)}) copy-start(f32[2048]{0:T(1024)} %param.30) | copy-start | bytes 24580
  231.5 34.9 %copy-start.3 = (f32[3,1408]{1,0:T(4,128)S(1)}, f32[3,1408]{1,0:T(4,128)}, u32[]{:S(2)}) copy-start(f32[3,1408]{1,0:T(4,128)} %param.34) | copy-start | bytes 50692
  231.5 34.9 %copy-start.4 = (f32[3,1408]{1,0:T(4,128)S(1)}, f32[3,1408]{1,0:T(4,128)}, u32[]{:S(2)}) copy-start(f32[3,1408]{1,0:T(4,128)} %param.33) | copy-start | bytes 50692
  237.9 14.3 %collective-permute-start = (bf16[256,2048]{1,0:T(8,128)(2,1)S(1)}, bf16[256,2048]{1,0:T(8,128)(2,1)S(1)}, u32[]{:S(2)}, u32[]{:S(2)}) collective-permute-start(bf16[256,2048]{1,0:T(8,128)(2,1)S(1)} %fusion.48), channel_id=1, source_target_pairs={{0,1},{1,2},{2,3},{3,0},{4,5},{5,6},{6,7},{7,4},{8,9},{9,10},{10,1... | collective-permute-start | bytes 3145736 | tf_op jit(solution)/shard_map/ppermute | solution.py:203
  238.0 340.9 %reduce-scatter.2.cloned.1.call-start = ((), (), s32[]{:S(2)}) async-start(), calls=%async_computation.6 | async-start | bytes 5242880 | tf_op jit(solution)/shard_map/reduce_scatter | solution.py:231
  252.1 14.2 %collective-permute-start.1 = (bf16[256,2048]{1,0:T(8,128)(2,1)S(1)}, bf16[256,2048]{1,0:T(8,128)(2,1)S(1)}, u32[]{:S(2)}, u32[]{:S(2)}) collective-permute-start(bf16[256,2048]{1,0:T(8,128)(2,1)S(1)} %collective-permute-done), channel_id=1, source_target_pairs={{0,1},{1,2},{2,3},{3,0},{4,5},{5,6},{6,7},{7,4},{8,9},{9,10},{10,1... | collective-permute-start | bytes 3145736 | tf_op jit(solution)/shard_map/ppermute | solution.py:203
  266.4 14.3 %collective-permute-start.2 = (bf16[256,2048]{1,0:T(8,128)(2,1)S(1)}, bf16[256,2048]{1,0:T(8,128)(2,1)}, u32[]{:S(2)}, u32[]{:S(2)}) collective-permute-start(bf16[256,2048]{1,0:T(8,128)(2,1)S(1)} %collective-permute-done.1), channel_id=1, source_target_pairs={{0,1},{1,2},{2,3},{3,0},{4,5},{5,6},{6,7},{7,4},{8,9},{9,10},{10,1... | collective-permute-start | bytes 3145736 | tf_op jit(solution)/shard_map/ppermute | solution.py:203
  284.3 43.1 %collective-permute-start.3 = (bf16[2,2048]{1,0:T(2,128)(2,1)S(1)}, bf16[2,2048]{1,0:T(2,128)(2,1)S(1)}, u32[]{:S(2)}, u32[]{:S(2)}) collective-permute-start(bf16[2,2048]{1,0:T(2,128)(2,1)S(1)} %constant_dynamic-slice_fusion.6), channel_id=1, source_target_pairs={{0,4},{4,8},{8,12},{12,16},{16,20},{20,24},{24,28},{1,5},{5,9},{9,... | collective-permute-start | bytes 24584 | tf_op jit(solution)/shard_map/ppermute | solution.py:35
Sparse Core Ops, SparseCore 0:
  119.8 43.0 all-gather.18
  164.5 65.4 all-gather.10
  232.2 95.1 all-gather.12
  329.4 90.4 all-gather.14
  421.9 91.3 all-gather.16
  536.0 42.7 reduce-scatter.1
